TPU v7x, 32 devices: a whole 2x2x4 slice. The times are simulated.
32 devices in a mesh: fs: 4 (over z), rep: 4 (over y, x), tp: 2 (over core).
Axes of the slice: x: 2, y: 2, z: 4, core: 2. Of those that a mesh axis runs over, the one named last changes fastest.
Arguments:
- first_mix: bfloat16 [12288, 2048], P(('fs', 'rep'), 'tp'), may hold values from -6 to 6
- second_mix: bfloat16 [12288, 2048], P(('fs', 'rep'), 'tp'), may hold values from -6 to 6
- lambda_head: float32 [8], P('tp'), may hold values from 0.3 to 0.8
- head_gain: float32 [256], replicated, may hold values from 0.1 to 1.9
- out_cotangent: bfloat16 [12288, 2048], P(('fs', 'rep')), may hold values from -0.053955078 to 0.053955078
- basis: bfloat16 [2048, 256], P('tp'), may hold values from -0.125 to 0.125
- weight: float32 [2048, 2048], P('tp', 'fs'), may hold values from -3 to 3
- first_moment: float32 [2048, 256], P('fs', 'tp'), may hold values from -4.5 to 4.5
- second_moment: float32 [2048, 256], P('fs', 'tp'), may hold values from 0.05 to 0.5
Outputs:
- weight_new: float32 [2048, 2048], P('tp', 'fs')
- weight_copy: bfloat16 [2048, 2048], P('tp')
- step_out: float32 [2048, 2048], P('tp', 'fs')
- first_new: float32 [2048, 256], P('fs', 'tp')
- second_new: float32 [2048, 256], P('fs', 'tp')
All inputs are finite; a program needn't handle non-finite values.
Results may differ from a plain program's by a relative error of at most 0.0075.
Values may be sent and summed in bfloat16 or wider, within the bound.
A program may use at most 64 MiB of HBM per device.

v0:
```python
import functools

import jax
import jax.numpy as jnp
from jax import lax
from jax.experimental import pallas as pl
from jax.experimental.pallas import tpu as pltpu
from jax.sharding import PartitionSpec as P

MESH = pl.DeviceIdType.MESH

vmem_grant = 67043328
out_scale = 0.8
beta_first = 0.9
beta_second = 0.95


def head_output(first_piece, second_piece, lambdas, head_gain):
    token_count = first_piece.shape[0]
    head_width = head_gain.shape[0]
    head_count = lambdas.shape[0] // head_width
    mixture = first_piece.astype(jnp.float32) - lambdas[None, :] * second_piece.astype(jnp.float32)
    grouped = mixture.reshape(token_count, head_count, head_width)
    inverse = lax.rsqrt(jnp.mean(grouped * grouped, axis=-1, keepdims=True) + 1e-06)
    normed = grouped * inverse * head_gain[None, None, :] * out_scale
    return normed.reshape(token_count, head_count * head_width).astype(jnp.bfloat16)


def split_product(narrow, wide, numbers):
    upper = wide.astype(jnp.bfloat16)
    lower = (wide - upper.astype(jnp.float32)).astype(jnp.bfloat16)
    return lax.dot_general(
        narrow, upper, numbers, preferred_element_type=jnp.float32
    ) + lax.dot_general(narrow, lower, numbers, preferred_element_type=jnp.float32)


def body(
    first_mix,
    second_mix,
    lambda_head,
    head_gain,
    out_cotangent,
    basis,
    weight,
    first_moment,
    second_moment,
):
    lambdas = jnp.repeat(lambda_head, head_gain.shape[0])
    head_out = head_output(first_mix, second_mix, lambdas, head_gain)
    reduced = jnp.dot(head_out, basis, preferred_element_type=jnp.float32)
    proj_rows = lax.psum_scatter(
        split_product(out_cotangent, reduced, (((0,), (0,)), ((), ()))),
        "fs",
        scatter_dimension=0,
        tiled=True,
    )
    proj_rows = lax.psum_scatter(proj_rows, "tp", scatter_dimension=1, tiled=True)
    projected = lax.psum(proj_rows, "rep")
    first_new = beta_first * first_moment + (1.0 - beta_first) * projected
    second_new = beta_second * second_moment + (1.0 - beta_second) * projected * projected
    direction = first_new / (jnp.sqrt(second_new) + 1e-08)
    energy = lax.psum(jnp.sum(direction * direction), ("fs", "tp"))
    entries = direction.shape[0] * direction.shape[1] * lax.axis_size("fs") * lax.axis_size("tp")
    spread = jnp.sqrt(energy / entries)
    full_direction = lax.all_gather(direction, "tp", axis=1, tiled=True)
    step_out = split_product(basis, full_direction, (((1,), (1,)), ((), ()))) * (
        -1.0 / (spread + 1e-06)
    )
    weight_new = weight + step_out
    weight_copy = lax.all_gather(weight_new.astype(jnp.bfloat16), "fs", axis=1, tiled=True)
    return (weight_new, weight_copy, step_out, first_new, second_new)


def exchange_kernel(
    axes,
    lambda_ref,
    gain_ref,
    first_hbm,
    second_hbm,
    cot_hbm,
    basis_hbm,
    weight_hbm,
    moment1_hbm,
    moment2_hbm,
    gathered_out,
    direction_out,
    projected_out,
    scale_out,
    first_v,
    second_v,
    cot_v,
    basis_v,
    weight_v,
    narrow_v,
    moment1_v,
    moment2_v,
    turned_v,
    mine_v,
    pair_send_v,
    pair_recv_v,
    plane_send_v,
    plane_recv_v,
    total_v,
    line_send_v,
    line_recv_v,
    projected_v,
    direction_v,
    joined_v,
    scale_v,
    load_sem,
    tile_sem,
    wz_send,
    wz_recv,
    wp_send,
    wp_recv,
    pair_send,
    pair_recv,
    plane_send,
    plane_recv,
    line_send,
    line_recv,
    proj_send,
    proj_recv,
    dz_send,
    dz_recv,
    dp_send,
    dp_recv,
    dt_send,
    dt_recv,
):
    line, plane = axes
    fs, rep, tp = lax.axis_index("fs"), lax.axis_index("rep"), lax.axis_index("tp")
    other = 1 - tp
    tokens, width = cot_v.shape
    half = direction_v.shape[-1]
    quarter = direction_v.shape[-2]
    shard = weight_v.shape[1]
    weight_rows = weight_v.shape[0]
    head_width = gain_ref.shape[1]
    heads = first_v.shape[1] // head_width
    tiles = tile_sem.shape[0]
    tile = tokens // tiles

    def ahead(at, step, count):
        return lax.rem(at + 1 + step, count)

    def behind(at, step, count):
        return lax.rem(at + count - 1 - step, count)

    fast_side = rep + 1 - 2 * lax.rem(rep, 2)
    slow_side = lax.rem(rep + 2, 4)
    peers = (3 - rep, slow_side, fast_side, rep)

    def remote(source, target, send, recv, where):
        return pltpu.make_async_remote_copy(
            src_ref=source,
            dst_ref=target,
            send_sem=send,
            recv_sem=recv,
            device_id=where,
            device_id_type=MESH,
        )

    my_rows = pl.ds(pl.multiple_of(rep * weight_rows, weight_rows), weight_rows)
    my_quarter = pl.ds(pl.multiple_of(rep * quarter, quarter), quarter)

    loads = [
        pltpu.make_async_copy(weight_hbm.at[my_rows], weight_v, load_sem.at[0]),
        pltpu.make_async_copy(
            basis_hbm.at[:, pl.ds(pl.multiple_of(tp * half, half), half)],
            basis_v.at[:, pl.ds(0, half)],
            load_sem.at[1],
        ),
        pltpu.make_async_copy(
            basis_hbm.at[:, pl.ds(pl.multiple_of(other * half, half), half)],
            basis_v.at[:, pl.ds(half, half)],
            load_sem.at[2],
        ),
        pltpu.make_async_copy(cot_hbm, cot_v, load_sem.at[3]),
        pltpu.make_async_copy(moment1_hbm.at[my_quarter], moment1_v, load_sem.at[4]),
        pltpu.make_async_copy(moment2_hbm.at[my_quarter], moment2_v, load_sem.at[5]),
    ]
    loads[0].start()
    loads[1].start()
    loads[2].start()
    tile_loads = []
    for t in range(tiles):
        rows = pl.ds(t * tile, tile)
        pieces = (
            pltpu.make_async_copy(first_hbm.at[rows], first_v.at[rows], tile_sem.at[t, 0]),
            pltpu.make_async_copy(second_hbm.at[rows], second_v.at[rows], tile_sem.at[t, 1]),
        )
        for piece in pieces:
            piece.start()
        tile_loads.append(pieces)
    for load in loads[3:]:
        load.start()

    barrier = pltpu.get_barrier_semaphore()
    for step in range(line - 1):
        pl.semaphore_signal(
            barrier, inc=1, device_id={"fs": ahead(fs, step, line)}, device_id_type=MESH
        )
    for step in range(plane - 1):
        pl.semaphore_signal(
            barrier, inc=1, device_id={"rep": peers[step]}, device_id_type=MESH
        )
    pl.semaphore_signal(barrier, inc=1, device_id={"tp": other}, device_id_type=MESH)
    pl.semaphore_wait(barrier, line + plane - 1)

    sends = []
    receives = []
    pair_receives = []
    proj_receives = []

    loads[0].wait()
    narrow_v[...] = weight_v[...].astype(jnp.bfloat16)
    weight_line = {}

    def send_line(step):
        copy = remote(
            narrow_v,
            gathered_out.at[fs, my_rows],
            wz_send.at[step],
            wz_recv.at[step],
            {"fs": ahead(fs, step, line)},
        )
        copy.start()
        weight_line[step] = copy
        sends.append(copy)

    early = (0, line - 2)
    late = tuple(range(1, line - 2))
    for step in early:
        send_line(step)

    side_copies = {}

    def pass_on(step):
        weight_line[step].wait_recv()
        here = gathered_out.at[behind(fs, step, line), my_rows]
        for side, peer in enumerate((slow_side, fast_side)):
            copy = remote(
                here, here, wp_send.at[step, side], wp_recv.at[step, side], {"rep": peer}
            )
            copy.start()
            sends.append(copy)
            side_copies[step, side] = copy

    def relay(step):
        source = behind(fs, step, line)
        part = weight_rows // 2
        for side, (origin, peer) in enumerate(((slow_side, fast_side), (fast_side, slow_side))):
            side_copies[step, side].wait_recv()
            start = pl.multiple_of(origin * weight_rows + side * part, part)
            here = gathered_out.at[source, pl.ds(start, part)]
            copy = remote(
                here, here, wp_send.at[step, 2 + side], wp_recv.at[step, 2 + side], {"rep": peer}
            )
            copy.start()
            sends.append(copy)
            receives.append(copy)

    loads[1].wait()
    loads[2].wait()
    gain = gain_ref[...] * out_scale
    for t in range(tiles):
        for piece in tile_loads[t]:
            piece.wait()
        rows = pl.ds(t * tile, tile)
        reduced = None
        for h in range(heads):
            lanes = pl.ds(h * head_width, head_width)
            mixture = first_v[rows, lanes].astype(jnp.float32) - lambda_ref[h] * second_v[
                rows, lanes
            ].astype(jnp.float32)
            inverse = lax.rsqrt(jnp.mean(mixture * mixture, axis=-1, keepdims=True) + 1e-06)
            normed = (mixture * inverse * gain).astype(jnp.bfloat16)
            term = jnp.dot(normed, basis_v[lanes, :], preferred_element_type=jnp.float32)
            reduced = term if reduced is None else reduced + term
        turned_v[:, rows] = reduced.T.astype(jnp.bfloat16)

    loads[3].wait()
    pair_copies = []
    plane_copies = []

    def pair_sum(step):
        pair_copies[step].wait_recv()
        return mine_v[step] + pair_recv_v[step]

    def send_plane(step):
        plane_send_v[step] = pair_sum(step).astype(jnp.bfloat16)
        copy = remote(
            plane_send_v.at[step],
            plane_recv_v.at[step],
            plane_send.at[step],
            plane_recv.at[step],
            {"rep": peers[step]},
        )
        copy.start()
        plane_copies.append(copy)
        sends.append(copy)

    for step in range(plane):
        part = peers[step]
        for at in range(line):
            start = pl.multiple_of(at * shard + part * quarter, quarter)
            product = jnp.dot(
                turned_v[...], cot_v[:, pl.ds(start, quarter)], preferred_element_type=jnp.float32
            )
            mine_v[step, at] = product[:half].T
            pair_send_v[step, at] = product[half:].T
        copy = remote(
            pair_send_v.at[step],
            pair_recv_v.at[step],
            pair_send.at[step],
            pair_recv.at[step],
            {"tp": other},
        )
        copy.start()
        pair_copies.append(copy)
        sends.append(copy)
        if step > 0:
            send_plane(step - 1)

    pass_on(0)
    total = pair_sum(plane - 1)
    for step in range(plane - 1):
        plane_copies[step].wait_recv()
        total = total + plane_recv_v[step].astype(jnp.float32)
    total_v[...] = total
    line_send_v[...] = total.astype(jnp.bfloat16)
    line_copies = []
    for step in range(line - 1):
        to = ahead(fs, step, line)
        copy = remote(
            line_send_v.at[to],
            line_recv_v.at[step],
            line_send.at[step],
            line_recv.at[step],
            {"fs": to},
        )
        copy.start()
        line_copies.append(copy)
        sends.append(copy)
    relay(0)
    pass_on(line - 2)
    projected = total_v[fs]
    for step in range(line - 1):
        line_copies[step].wait_recv()
        projected = projected + line_recv_v[step].astype(jnp.float32)
    projected_v[rep] = projected
    loads[4].wait()
    loads[5].wait()
    first_new = beta_first * moment1_v[...] + (1.0 - beta_first) * projected
    second_new = beta_second * moment2_v[...] + (1.0 - beta_second) * projected * projected
    direction = first_new / (jnp.sqrt(second_new) + 1e-08)
    direction_v[tp, fs, rep] = direction.astype(jnp.bfloat16)
    direction_line = []
    for step in range(line - 1):
        here = direction_v.at[tp, fs, rep]
        copy = remote(
            here, here, dz_send.at[step], dz_recv.at[step], {"fs": ahead(fs, step, line)}
        )
        copy.start()
        direction_line.append(copy)
        sends.append(copy)
    for step in late:
        send_line(step)
    for step in range(plane - 1):
        here = projected_v.at[rep]
        copy = remote(
            here, here, proj_send.at[step], proj_recv.at[step], {"rep": peers[step]}
        )
        copy.start()
        sends.append(copy)
        proj_receives.append(copy)
    for copy in direction_line:
        copy.wait_recv()
    direction_plane = []
    for step in range(plane - 1):
        here = direction_v.at[tp, :, rep]
        copy = remote(
            here, here, dp_send.at[step], dp_recv.at[step], {"rep": peers[step]}
        )
        copy.start()
        direction_plane.append(copy)
        sends.append(copy)

    def to_pair(step, part):
        here = direction_v.at[tp, :, part]
        copy = remote(here, here, dt_send.at[step], dt_recv.at[step], {"tp": other})
        copy.start()
        sends.append(copy)
        pair_receives.append(copy)

    to_pair(plane - 1, rep)
    for step in range(plane - 1):
        direction_plane[step].wait_recv()
        to_pair(step, peers[step])
    relay(line - 2)
    for step in late:
        pass_on(step)
    for copy in pair_receives:
        copy.wait_recv()
    energy = jnp.zeros((1, half), jnp.float32)
    for side in range(2):
        piece = direction_v[side].reshape(width, half)
        wide = piece.astype(jnp.float32)
        joined_v[side * half : (side + 1) * half, :] = wide.T.astype(jnp.bfloat16)
        energy += jnp.sum(wide * wide, axis=0, keepdims=True)
    spread = jnp.sqrt(jnp.sum(energy, axis=1, keepdims=True) / (width * 2 * half))
    scale_v[...] = jnp.broadcast_to(-1.0 / (spread + 1e-06), scale_v.shape)
    for step in late:
        relay(step)
    for copy in proj_receives:
        copy.wait_recv()
    outs = [
        pltpu.make_async_copy(joined_v, direction_out, load_sem.at[0]),
        pltpu.make_async_copy(projected_v, projected_out, load_sem.at[1]),
        pltpu.make_async_copy(scale_v, scale_out, load_sem.at[2]),
    ]
    for copy in outs:
        copy.start()
    for copy in receives:
        copy.wait_recv()
    for copy in sends:
        copy.wait_send()
    for copy in outs:
        copy.wait()


def update_kernel(
    line,
    basis_ref,
    direction_ref,
    scale_ref,
    projected_ref,
    moment1_ref,
    moment2_ref,
    weight_ref,
    gathered_ref,
    weight_new_ref,
    copy_ref,
    step_ref,
    first_new_ref,
    second_new_ref,
):
    fs = lax.axis_index("fs")
    shard = weight_ref.shape[1]
    projected = projected_ref[...]
    first_new_ref[...] = beta_first * moment1_ref[...] + (1.0 - beta_first) * projected
    second_new_ref[...] = (
        beta_second * moment2_ref[...] + (1.0 - beta_second) * projected * projected
    )
    scale = scale_ref[0:1, 0:1]
    basis = basis_ref[...]
    for at in range(line):
        columns = pl.ds(at * shard, shard)
        step = (
            jnp.dot(basis, direction_ref[:, columns], preferred_element_type=jnp.float32)
            * scale
        )

        @pl.when(fs == at)
        def _():
            fresh = weight_ref[...] + step
            step_ref[...] = step
            weight_new_ref[...] = fresh
            copy_ref[:, columns] = fresh.astype(jnp.bfloat16)

        @pl.when(fs != at)
        def _():
            copy_ref[:, columns] = (gathered_ref[at].astype(jnp.float32) + step).astype(
                jnp.bfloat16
            )


def fast_body(
    sizes,
    first_mix,
    second_mix,
    lambda_head,
    head_gain,
    out_cotangent,
    basis,
    weight,
    first_moment,
    second_moment,
):
    line, plane = sizes
    tokens, width = out_cotangent.shape
    values, rank = basis.shape
    shard, half = first_moment.shape
    quarter = shard // plane
    rows = values // plane
    tile = 256 if tokens % 256 == 0 else tokens
    tiles = tokens // tile
    any_space = pl.BlockSpec(memory_space=pl.ANY)
    dma = pltpu.SemaphoreType.DMA
    f32, bf16 = jnp.float32, jnp.bfloat16
    gathered, direction, projected, scale = pl.pallas_call(
        functools.partial(exchange_kernel, sizes),
        out_shape=(
            jax.ShapeDtypeStruct((line, values, shard), bf16),
            jax.ShapeDtypeStruct((rank, width), bf16),
            jax.ShapeDtypeStruct((plane, quarter, half), f32),
            jax.ShapeDtypeStruct((8, 128), f32),
        ),
        in_specs=[
            pl.BlockSpec(memory_space=pltpu.SMEM),
            pl.BlockSpec(memory_space=pltpu.VMEM),
        ]
        + [any_space] * 7,
        out_specs=(any_space,) * 4,
        scratch_shapes=[
            pltpu.VMEM(first_mix.shape, bf16),
            pltpu.VMEM(second_mix.shape, bf16),
            pltpu.VMEM(out_cotangent.shape, bf16),
            pltpu.VMEM(basis.shape, bf16),
            pltpu.VMEM((rows, shard), f32),
            pltpu.VMEM((rows, shard), bf16),
            pltpu.VMEM((quarter, half), f32),
            pltpu.VMEM((quarter, half), f32),
            pltpu.VMEM((rank, tokens), bf16),
            pltpu.VMEM((plane, line, quarter, half), f32),
            pltpu.VMEM((plane, line, quarter, half), f32),
            pltpu.VMEM((plane, line, quarter, half), f32),
            pltpu.VMEM((plane - 1, line, quarter, half), bf16),
            pltpu.VMEM((plane - 1, line, quarter, half), bf16),
            pltpu.VMEM((line, quarter, half), f32),
            pltpu.VMEM((line, quarter, half), bf16),
            pltpu.VMEM((line - 1, quarter, half), bf16),
            pltpu.VMEM((plane, quarter, half), f32),
            pltpu.VMEM((2, line, plane, quarter, half), bf16),
            pltpu.VMEM((rank, width), bf16),
            pltpu.VMEM((8, 128), f32),
            dma((6,)),
            dma((tiles, 2)),
            dma((line - 1,)),
            dma((line - 1,)),
            dma((line - 1, 4)),
            dma((line - 1, 4)),
            dma((plane,)),
            dma((plane,)),
            dma((plane - 1,)),
            dma((plane - 1,)),
            dma((line - 1,)),
            dma((line - 1,)),
            dma((plane - 1,)),
            dma((plane - 1,)),
            dma((line - 1,)),
            dma((line - 1,)),
            dma((plane - 1,)),
            dma((plane - 1,)),
            dma((plane,)),
            dma((plane,)),
        ],
        compiler_params=pltpu.CompilerParams(
            collective_id=0, has_side_effects=True, vmem_limit_bytes=vmem_grant
        ),
    )(
        lambda_head,
        head_gain.reshape(1, -1),
        first_mix,
        second_mix,
        out_cotangent,
        basis,
        weight,
        first_moment,
        second_moment,
    )
    blocks = 2
    block = values // blocks
    moment_block = shard // blocks
    whole = lambda *shape: pl.BlockSpec(shape, lambda i: (0,) * len(shape))
    mrow = pl.BlockSpec((moment_block, half), lambda i: (i, 0))
    rowed = lambda columns: pl.BlockSpec((block, columns), lambda i: (i, 0))
    return pl.pallas_call(
        functools.partial(update_kernel, line),
        grid=(values // block,),
        out_shape=(
            jax.ShapeDtypeStruct(weight.shape, f32),
            jax.ShapeDtypeStruct((values, width), bf16),
            jax.ShapeDtypeStruct(weight.shape, f32),
            jax.ShapeDtypeStruct(first_moment.shape, f32),
            jax.ShapeDtypeStruct(first_moment.shape, f32),
        ),
        in_specs=[
            rowed(rank),
            whole(rank, width),
            whole(8, 128),
            mrow,
            mrow,
            mrow,
            rowed(shard),
            pl.BlockSpec((line, block, shard), lambda i: (0, i, 0)),
        ],
        out_specs=(
            rowed(shard),
            rowed(width),
            rowed(shard),
            mrow,
            mrow,
        ),
        compiler_params=pltpu.CompilerParams(vmem_limit_bytes=vmem_grant),
    )(
        basis,
        direction,
        scale,
        projected.reshape(shard, half),
        first_moment,
        second_moment,
        weight,
        gathered,
    )


def solution(mesh):
    line, plane, pair = (mesh.shape[name] for name in ("fs", "rep", "tp"))

    def chosen(*args):
        basis, first_moment = args[5], args[7]
        quarter_fits = first_moment.shape[0] % (plane * 128) == 0
        rows_fit = basis.shape[0] % (plane * 16) == 0 and basis.shape[0] % 64 == 0
        rank_fits = pair == 2 and first_moment.shape[1] % 128 == 0
        if line > 2 and plane == 4 and quarter_fits and rows_fit and rank_fits:
            return fast_body((line, plane), *args)
        return body(*args)

    return jax.shard_map(
        chosen,
        mesh=mesh,
        in_specs=(
            P(("fs", "rep"), "tp"),
            P(("fs", "rep"), "tp"),
            P("tp"),
            P(),
            P(("fs", "rep"), None),
            P("tp", None),
            P("tp", "fs"),
            P("fs", "tp"),
            P("fs", "tp"),
        ),
        out_specs=(P("tp", "fs"), P("tp", None), P("tp", "fs"), P("fs", "tp"), P("fs", "tp")),
        check_vma=False,
    )
```

profile of v0, /device:TPU:0, one launch (start us, length us, event | category | flops | bytes accessed | tf_op | source)
XLA Modules:
  0.0 66.7 jit_solution(7215975111016463102)
XLA Ops:
  0.6 58.2 %shard_map.128 = (bf16[4,1024,512]{2,1,0:T(8,128)(2,1)}, bf16[256,2048]{1,0:T(8,128)(2,1)}, f32[4,128,128]{2,1,0:T(8,128)}, f32[8,128]{1,0:T(8,128)}) custom-call(f32[4]{0:T(128)} %lambda_ref.1, f32[1,256]{1,0:T(1,128)} %bitcast.3, bf16[768,1024]{1,0:T(8,128)(2,1)} %first_hbm.1, bf16[768,1024]{1,0:T(8,128)(2,1)} %second_hbm.1, bf16[768,2048]{1,0:T(8,128)(2,1)} %cot_hbm.1, ...), custom_call_target="tpu_custom_call" | custom-call | tf_op jit(solution)/shard_map/pallas_call | solution.py:502
  58.8 7.9 %shard_map.129 = (f32[1024,512]{1,0:T(8,128)}, bf16[1024,2048]{1,0:T(8,128)(2,1)}, f32[1024,512]{1,0:T(8,128)}, f32[512,128]{1,0:T(8,128)}, f32[512,128]{1,0:T(8,128)}) custom-call(bf16[1024,256]{1,0:T(8,128)(2,1)} %basis_ref.1, bf16[256,2048]{1,0:T(8,128)(2,1)} %get-tuple-element.9.direction_ref, f32[8,128]{1,0:T(8,128)} %get-tuple-element.10.scale_ref, ...), custom_call_target="tpu_custom_call" | custom-call | tf_op jit(solution)/shard_map/pallas_call | solution.py:579
where the time goes:
time: 66.9 us; the launch traced here: 66.7 us
  Pallas kernels  66.1 us (99%)
    pallas_call x1, Pallas kernels, fast_body(): pl.pallas_call(functools.partial(exchange_kernel, sizes), out_shape=(jax....  58.2 us
    pallas_call x1, Pallas kernels, fast_body(): pl.pallas_call(functools.partial(update_kernel, line), grid=(values // bl...  7.92 us

commit v1 on v0

v1 whole, which is shorter than its diff:
```python
import functools

import jax
import jax.numpy as jnp
from jax import lax
from jax.experimental import pallas as pl
from jax.experimental.pallas import tpu as pltpu
from jax.sharding import PartitionSpec as P

MESH = pl.DeviceIdType.MESH

vmem_grant = 67043328
out_scale = 0.8
beta_first = 0.9
beta_second = 0.95
quarter_chunks = 4
extra_part = 8


def head_output(first_piece, second_piece, lambdas, head_gain):
    token_count = first_piece.shape[0]
    head_width = head_gain.shape[0]
    head_count = lambdas.shape[0] // head_width
    mixture = first_piece.astype(jnp.float32) - lambdas[None, :] * second_piece.astype(jnp.float32)
    grouped = mixture.reshape(token_count, head_count, head_width)
    inverse = lax.rsqrt(jnp.mean(grouped * grouped, axis=-1, keepdims=True) + 1e-06)
    normed = grouped * inverse * head_gain[None, None, :] * out_scale
    return normed.reshape(token_count, head_count * head_width).astype(jnp.bfloat16)


def split_product(narrow, wide, numbers):
    upper = wide.astype(jnp.bfloat16)
    lower = (wide - upper.astype(jnp.float32)).astype(jnp.bfloat16)
    return lax.dot_general(
        narrow, upper, numbers, preferred_element_type=jnp.float32
    ) + lax.dot_general(narrow, lower, numbers, preferred_element_type=jnp.float32)


def body(
    first_mix,
    second_mix,
    lambda_head,
    head_gain,
    out_cotangent,
    basis,
    weight,
    first_moment,
    second_moment,
):
    lambdas = jnp.repeat(lambda_head, head_gain.shape[0])
    head_out = head_output(first_mix, second_mix, lambdas, head_gain)
    reduced = jnp.dot(head_out, basis, preferred_element_type=jnp.float32)
    proj_rows = lax.psum_scatter(
        split_product(out_cotangent, reduced, (((0,), (0,)), ((), ()))),
        "fs",
        scatter_dimension=0,
        tiled=True,
    )
    proj_rows = lax.psum_scatter(proj_rows, "tp", scatter_dimension=1, tiled=True)
    projected = lax.psum(proj_rows, "rep")
    first_new = beta_first * first_moment + (1.0 - beta_first) * projected
    second_new = beta_second * second_moment + (1.0 - beta_second) * projected * projected
    direction = first_new / (jnp.sqrt(second_new) + 1e-08)
    energy = lax.psum(jnp.sum(direction * direction), ("fs", "tp"))
    entries = direction.shape[0] * direction.shape[1] * lax.axis_size("fs") * lax.axis_size("tp")
    spread = jnp.sqrt(energy / entries)
    full_direction = lax.all_gather(direction, "tp", axis=1, tiled=True)
    step_out = split_product(basis, full_direction, (((1,), (1,)), ((), ()))) * (
        -1.0 / (spread + 1e-06)
    )
    weight_new = weight + step_out
    weight_copy = lax.all_gather(weight_new.astype(jnp.bfloat16), "fs", axis=1, tiled=True)
    return (weight_new, weight_copy, step_out, first_new, second_new)


def exchange_kernel(
    sizes,
    lambda_ref,
    gain_ref,
    first_hbm,
    second_hbm,
    cot_hbm,
    basis_hbm,
    weight_hbm,
    moment1_hbm,
    moment2_hbm,
    copy_ref,
    new_ref,
    step_ref,
    first_new_ref,
    second_new_ref,
    first_v,
    second_v,
    cot_v,
    basis_v,
    weight_v,
    gathered_v,
    moment1_v,
    moment2_v,
    half_mine_v,
    half_send_v,
    half_recv_v,
    turned_v,
    mine_v,
    plane_send_v,
    plane_recv_v,
    line_send_v,
    line_recv_v,
    projected_v,
    direction_v,
    joined_v,
    load_sem,
    tile_sem,
    wz_send,
    wf_send,
    wz_recv,
    wp_send,
    wp_recv,
    wr_send,
    wr_recv,
    half_send,
    half_recv,
    plane_send,
    plane_recv,
    line_send,
    line_recv,
    proj_send,
    proj_recv,
    dz_send,
    dz_recv,
    dp_send,
    dp_recv,
    dt_send,
    dt_recv,
):
    line, plane = sizes
    fs, rep, tp = lax.axis_index("fs"), lax.axis_index("rep"), lax.axis_index("tp")
    other = 1 - tp
    tokens, width = cot_v.shape
    half, quarter = direction_v.shape[-2:]
    values, shard = weight_v.shape
    quarter_rows = values // plane
    chunk = quarter_rows // quarter_chunks
    head_width = gain_ref.shape[1]
    heads = first_v.shape[1] // head_width
    tiles = tile_sem.shape[0]
    tile = tokens // tiles

    fast_side = rep + 1 - 2 * lax.rem(rep, 2)
    slow_side = lax.rem(rep + 2, 4)
    far_side = 3 - rep
    sides = (fast_side, slow_side)
    peers = (far_side, slow_side, fast_side, rep)

    near_source = 1 + lax.rem(fs, 2)
    last_source = jnp.where(fs < 2, 3, 0)
    sources = (near_source, 6 - fs - near_source - last_source, last_source)
    nexts = tuple(jnp.where(source < fs, fs + 1, fs - 1) for source in sources)
    goes_on = tuple((to >= 0) & (to < line) for to in nexts)

    def remote(source, target, send, recv, where):
        return pltpu.make_async_remote_copy(
            src_ref=source,
            dst_ref=target,
            send_sem=send,
            recv_sem=recv,
            device_id=where,
            device_id_type=MESH,
        )

    def rows_of(owner, start, size):
        return pl.ds(pl.multiple_of(owner * quarter_rows + start, 16), size)

    def weight_load(owner, at):
        rows = rows_of(owner, 0, quarter_rows)
        return pltpu.make_async_copy(weight_hbm.at[rows], weight_v.at[rows], load_sem.at[at])

    weight_loads = [weight_load(owner, at) for at, owner in enumerate((rep, far_side) + sides)]
    basis_loads = [
        pltpu.make_async_copy(
            basis_hbm.at[:, pl.ds(pl.multiple_of(side * half, half), half)],
            basis_v.at[:, pl.ds(at * half, half)],
            load_sem.at[4 + at],
        )
        for at, side in enumerate((tp, other))
    ]
    cot_load = pltpu.make_async_copy(cot_hbm, cot_v, load_sem.at[6])
    moment_loads = [
        pltpu.make_async_copy(moment1_hbm, moment1_v, load_sem.at[7]),
        pltpu.make_async_copy(moment2_hbm, moment2_v, load_sem.at[8]),
    ]
    weight_loads[0].start()
    for load in basis_loads:
        load.start()
    tile_loads = []
    for t in range(tiles):
        rows = pl.ds(t * tile, tile)
        pieces = (
            pltpu.make_async_copy(first_hbm.at[rows], first_v.at[rows], tile_sem.at[t, 0]),
            pltpu.make_async_copy(second_hbm.at[rows], second_v.at[rows], tile_sem.at[t, 1]),
        )
        for piece in pieces:
            piece.start()
        tile_loads.append(pieces)
    cot_load.start()
    weight_loads[1].start()
    for load in moment_loads + weight_loads[2:]:
        load.start()

    barrier = pltpu.get_barrier_semaphore()
    for step in range(1, line):
        pl.semaphore_signal(
            barrier, inc=1, device_id={"fs": lax.rem(fs + step, line)}, device_id_type=MESH
        )
    for step in range(plane - 1):
        pl.semaphore_signal(
            barrier, inc=1, device_id={"rep": peers[step]}, device_id_type=MESH
        )
    pl.semaphore_signal(barrier, inc=1, device_id={"tp": other}, device_id_type=MESH)
    pl.semaphore_wait(barrier, line + plane - 1)

    sends = []
    guarded = []

    extra = quarter_rows * extra_part // 16
    rest = (quarter_rows - extra) // 2
    pieces = [(rep, c * chunk, chunk) for c in range(quarter_chunks)]
    pieces += [(far_side, c * (extra // 2), extra // 2) for c in range(2)]
    quarters = tuple(range(quarter_chunks))
    extras = (quarter_chunks, quarter_chunks + 1)

    def line_copy(source, c, send, to):
        here = gathered_v.at[source, rows_of(*pieces[c])]
        return remote(here, here, send, wz_recv.at[source, c], {"fs": to})

    def start_if(wanted, copy):
        @pl.when(wanted)
        def _():
            copy.start()

        guarded.append((wanted, copy))

    def narrow(c):
        rows = rows_of(*pieces[c])
        gathered_v[fs, rows] = weight_v[rows].astype(jnp.bfloat16)

    def send_own(c):
        start_if(fs < line - 1, line_copy(fs, c, wz_send.at[0, c], fs + 1))
        start_if(fs > 0, line_copy(fs, c, wz_send.at[1, c], fs - 1))

    def arrive(t, c):
        copy = line_copy(sources[t], c, wf_send.at[t, c], nexts[t])
        copy.wait_recv()
        start_if(goes_on[t], copy)
        if c in quarters:
            here = gathered_v.at[sources[t], rows_of(*pieces[c])]
            for side in range(2):
                copy = remote(
                    here,
                    here,
                    wp_send.at[t, c, side],
                    wp_recv.at[t, c, side],
                    {"rep": sides[side]},
                )
                copy.start()
                sends.append(copy)

    waited = set()

    def from_side(t, c, side):
        if (t, c, side) not in waited:
            waited.add((t, c, side))
            here = gathered_v.at[sources[t], rows_of(sides[side], c * chunk, chunk)]
            remote(
                here,
                here,
                wp_send.at[t, c, side],
                wp_recv.at[t, c, side],
                {"rep": sides[side]},
            ).wait_recv()

    def relay_copy(t, side, owner):
        here = gathered_v.at[sources[t], rows_of(owner, extra + side * rest, rest)]
        return remote(
            here, here, wr_send.at[t, side], wr_recv.at[t, side], {"rep": sides[1 - side]}
        )

    def relay(t):
        for side in range(2):
            from_side(t, (extra + side * rest) // chunk, side)
            copy = relay_copy(t, side, sides[side])
            copy.start()
            sends.append(copy)

    def finish(t):
        for c in quarters:
            for side in range(2):
                from_side(t, c, side)
        for side in range(2):
            relay_copy(t, side, far_side).wait_recv()

    weight_loads[0].wait()
    for c in quarters:
        narrow(c)
        send_own(c)

    for load in basis_loads:
        load.wait()
    gain = gain_ref[...] * out_scale
    half_copies = []

    def join_pair(t):
        half_copies[t].wait_recv()
        both = half_mine_v[t] + half_recv_v[t]
        turned_v[:, t * tile : (t + 1) * tile] = both.T.astype(jnp.bfloat16)

    for t in range(tiles):
        for piece in tile_loads[t]:
            piece.wait()
        rows = pl.ds(t * tile, tile)
        reduced = None
        for h in range(heads):
            lanes = pl.ds(h * head_width, head_width)
            mixture = first_v[rows, lanes].astype(jnp.float32) - lambda_ref[h] * second_v[
                rows, lanes
            ].astype(jnp.float32)
            inverse = lax.rsqrt(jnp.mean(mixture * mixture, axis=-1, keepdims=True) + 1e-06)
            normed = (mixture * inverse * gain).astype(jnp.bfloat16)
            term = jnp.dot(normed, basis_v[lanes, :], preferred_element_type=jnp.float32)
            reduced = term if reduced is None else reduced + term
        half_mine_v[t] = reduced[:, :half]
        half_send_v[t] = reduced[:, half:]
        copy = remote(
            half_send_v.at[t],
            half_recv_v.at[t],
            half_send.at[t],
            half_recv.at[t],
            {"tp": other},
        )
        copy.start()
        half_copies.append(copy)
        sends.append(copy)
        if t > 0:
            join_pair(t - 1)
    cot_load.wait()
    arrive(0, 0)
    join_pair(tiles - 1)

    order = (2, 1, 3, 0)
    plane_copies = {}
    for ahead in order:
        at = lax.rem(fs + ahead, line)
        product = jnp.dot(
            turned_v[...],
            cot_v[:, pl.ds(pl.multiple_of(at * shard, shard), shard)],
            preferred_element_type=jnp.float32,
        )
        for part in range(plane):
            piece = product[:, part * quarter : (part + 1) * quarter]
            mine_v[ahead, part] = piece
            plane_send_v[ahead, part] = piece.astype(jnp.bfloat16)
        for step in range(plane - 1):
            copy = remote(
                plane_send_v.at[ahead, peers[step]],
                plane_recv_v.at[step, ahead],
                plane_send.at[step, ahead],
                plane_recv.at[step, ahead],
                {"rep": peers[step]},
            )
            copy.start()
            plane_copies[step, ahead] = copy
            sends.append(copy)

    for c in quarters[1:]:
        arrive(0, c)
    weight_loads[1].wait()
    for c in extras:
        narrow(c)
    for load in moment_loads:
        load.wait()
    my_quarter = pl.ds(pl.multiple_of(rep * quarter, quarter), quarter)
    moment1 = moment1_v[my_quarter].T
    moment2 = moment2_v[my_quarter].T

    line_copies = []
    for ahead in order:
        total = mine_v[ahead, rep]
        for step in range(plane - 1):
            plane_copies[step, ahead].wait_recv()
            total = total + plane_recv_v[step, ahead].astype(jnp.float32)
        if ahead:
            line_send_v[ahead] = total.astype(jnp.bfloat16)
            copy = remote(
                line_send_v.at[ahead],
                line_recv_v.at[ahead],
                line_send.at[ahead],
                line_recv.at[ahead],
                {"fs": lax.rem(fs + ahead, line)},
            )
            copy.start()
            line_copies.append(copy)
            sends.append(copy)

    for c in extras:
        send_own(c)
    for c in quarters[:2]:
        arrive(1, c)

    projected = total
    for copy, ahead in zip(line_copies, order):
        copy.wait_recv()
        projected = projected + line_recv_v[ahead].astype(jnp.float32)
    first_new = beta_first * moment1 + (1.0 - beta_first) * projected
    second_new = beta_second * moment2 + (1.0 - beta_second) * projected * projected
    direction = first_new / (jnp.sqrt(second_new) + 1e-08)
    direction_v[tp, fs, rep] = direction.astype(jnp.bfloat16)
    projected_v[rep] = projected.astype(jnp.bfloat16)

    def spread_line(source, to, at):
        here = direction_v.at[tp, source, rep]
        return remote(here, here, dz_send.at[at], dz_recv.at[source], {"fs": to})

    plane_directions = {}

    def spread_plane(at, source):
        for step in range(plane - 1):
            here = direction_v.at[tp, source, rep]
            copy = remote(
                here, here, dp_send.at[at, step], dp_recv.at[at, step], {"rep": peers[step]}
            )
            copy.start()
            sends.append(copy)

    def to_pair(at, source):
        for step in range(plane - 1):
            here = direction_v.at[tp, source, peers[step]]
            remote(
                here, here, dp_send.at[at, step], dp_recv.at[at, step], {"rep": peers[step]}
            ).wait_recv()
        here = direction_v.at[tp, source]
        copy = remote(here, here, dt_send.at[at], dt_recv.at[at], {"tp": other})
        copy.start()
        sends.append(copy)

    for at, to in enumerate(sources):
        copy = spread_line(fs, to, at)
        copy.start()
        sends.append(copy)
    spread_plane(3, fs)
    proj_copies = []
    for step in range(plane - 1):
        here = projected_v.at[rep]
        copy = remote(
            here, here, proj_send.at[step], proj_recv.at[step], {"rep": peers[step]}
        )
        copy.start()
        sends.append(copy)
        proj_copies.append(copy)

    for c in quarters[2:]:
        arrive(1, c)
    for at, source in enumerate(sources):
        spread_line(source, source, at).wait_recv()
        spread_plane(at, source)
    relay(0)
    for c in quarters:
        arrive(2, c)
    for c in extras:
        arrive(0, c)
    to_pair(3, fs)
    for at, source in enumerate(sources):
        to_pair(at, source)
    relay(1)
    for c in extras:
        arrive(1, c)
    for c in extras:
        arrive(2, c)
    relay(2)

    for load in weight_loads[2:]:
        load.wait()
    for at, source in enumerate(sources + (fs,)):
        here = direction_v.at[other, source]
        remote(here, here, dt_send.at[at], dt_recv.at[at], {"tp": other}).wait_recv()
    energy = jnp.zeros((half, quarter), jnp.float32)
    for at in range(line):
        for part in range(plane):
            lanes = pl.ds((at * plane + part) * quarter, quarter)
            for side in range(2):
                wide = direction_v[side, at, part].astype(jnp.float32)
                energy += wide * wide
            joined_v[:half, lanes] = direction_v[tp, at, part]
            joined_v[half:, lanes] = direction_v[other, at, part]
    total = jnp.sum(jnp.sum(energy, axis=0, keepdims=True), axis=1, keepdims=True)
    spread = jnp.sqrt(total / (width * 2 * half))
    scale = -1.0 / (spread + 1e-06)

    block = values // 4

    def step_block(at, rows):
        return (
            jnp.dot(
                basis_v[rows, :],
                joined_v[:, pl.ds(pl.multiple_of(at * shard, shard), shard)],
                preferred_element_type=jnp.float32,
            )
            * scale
        )

    def columns_of(at):
        return pl.ds(pl.multiple_of(at * shard, shard), shard)

    for b in range(4):
        rows = pl.ds(b * block, block)
        step = step_block(fs, rows)
        fresh = weight_v[rows, :] + step
        step_ref[rows, :] = step
        new_ref[rows, :] = fresh
        copy_ref[rows, columns_of(fs)] = fresh.astype(jnp.bfloat16)
    for copy in proj_copies:
        copy.wait_recv()
    for part in range(plane):
        rows = pl.ds(part * quarter, quarter)
        piece = projected_v[part].astype(jnp.float32).T
        first_new_ref[rows, :] = beta_first * moment1_v[rows, :] + (1.0 - beta_first) * piece
        second_new_ref[rows, :] = (
            beta_second * moment2_v[rows, :] + (1.0 - beta_second) * piece * piece
        )
    for t, source in enumerate(sources):
        finish(t)
        for b in range(4):
            rows = pl.ds(b * block, block)
            copy_ref[rows, columns_of(source)] = (
                gathered_v[source, rows].astype(jnp.float32) + step_block(source, rows)
            ).astype(jnp.bfloat16)
    for copy in sends:
        copy.wait_send()
    for wanted, copy in guarded:

        @pl.when(wanted)
        def _():
            copy.wait_send()


def store_kernel(*refs):
    count = (len(refs) - 1) // 2
    sources, targets, store_sem = refs[:count], refs[count : 2 * count], refs[-1]
    copies = []
    for at in range(count):
        parts = store_sem.shape[1]
        rows = sources[at].shape[0] // parts
        for part in range(parts):
            here = pl.ds(part * rows, rows)
            copies.append(
                pltpu.make_async_copy(
                    sources[at].at[here], targets[at].at[here], store_sem.at[at, part]
                )
            )
    for copy in copies:
        copy.start()
    for copy in copies:
        copy.wait()


def fast_body(
    sizes,
    first_mix,
    second_mix,
    lambda_head,
    head_gain,
    out_cotangent,
    basis,
    weight,
    first_moment,
    second_moment,
):
    line, plane = sizes
    tokens, width = out_cotangent.shape
    values, rank = basis.shape
    shard, half = first_moment.shape
    quarter = shard // plane
    tile = 256 if tokens % 256 == 0 else tokens
    tiles = tokens // tile
    pieces = quarter_chunks + 2
    any_space = pl.BlockSpec(memory_space=pl.ANY)
    on_chip = pl.BlockSpec(memory_space=pltpu.VMEM)
    dma = pltpu.SemaphoreType.DMA
    f32, bf16 = jnp.float32, jnp.bfloat16
    shapes = (
        ((values, width), bf16),
        (weight.shape, f32),
        (weight.shape, f32),
        (first_moment.shape, f32),
        (first_moment.shape, f32),
    )
    held = sum(jnp.dtype(kind).itemsize * shape[0] * shape[1] for shape, kind in shapes)
    fresh = pl.pallas_call(
        functools.partial(exchange_kernel, sizes),
        out_shape=tuple(pltpu.VMEM(shape, kind) for shape, kind in shapes),
        in_specs=[pl.BlockSpec(memory_space=pltpu.SMEM), on_chip] + [any_space] * 7,
        out_specs=(on_chip,) * 5,
        scratch_shapes=[
            pltpu.VMEM(first_mix.shape, bf16),
            pltpu.VMEM(second_mix.shape, bf16),
            pltpu.VMEM(out_cotangent.shape, bf16),
            pltpu.VMEM(basis.shape, bf16),
            pltpu.VMEM(weight.shape, f32),
            pltpu.VMEM((line, values, shard), bf16),
            pltpu.VMEM(first_moment.shape, f32),
            pltpu.VMEM(first_moment.shape, f32),
            pltpu.VMEM((tiles, tile, half), f32),
            pltpu.VMEM((tiles, tile, half), f32),
            pltpu.VMEM((tiles, tile, half), f32),
            pltpu.VMEM((half, tokens), bf16),
            pltpu.VMEM((line, plane, half, quarter), f32),
            pltpu.VMEM((line, plane, half, quarter), bf16),
            pltpu.VMEM((plane - 1, line, half, quarter), bf16),
            pltpu.VMEM((line, half, quarter), bf16),
            pltpu.VMEM((line, half, quarter), bf16),
            pltpu.VMEM((plane, half, quarter), bf16),
            pltpu.VMEM((2, line, plane, half, quarter), bf16),
            pltpu.VMEM((rank, width), bf16),
            dma((9,)),
            dma((tiles, 2)),
            dma((2, pieces)),
            dma((line - 1, pieces)),
            dma((line, pieces)),
            dma((line - 1, quarter_chunks, 2)),
            dma((line - 1, quarter_chunks, 2)),
            dma((line - 1, 2)),
            dma((line - 1, 2)),
            dma((tiles,)),
            dma((tiles,)),
            dma((plane - 1, line)),
            dma((plane - 1, line)),
            dma((line,)),
            dma((line,)),
            dma((plane - 1,)),
            dma((plane - 1,)),
            dma((line - 1,)),
            dma((line,)),
            dma((line, plane - 1)),
            dma((line, plane - 1)),
            dma((line,)),
            dma((line,)),
        ],
        compiler_params=pltpu.CompilerParams(
            collective_id=0, has_side_effects=True, vmem_limit_bytes=vmem_grant - held
        ),
    )(
        lambda_head,
        head_gain.reshape(1, -1),
        first_mix,
        second_mix,
        out_cotangent,
        basis,
        weight,
        first_moment,
        second_moment,
    )
    copied, new, step, first_new, second_new = pl.pallas_call(
        store_kernel,
        out_shape=tuple(jax.ShapeDtypeStruct(shape, kind) for shape, kind in shapes),
        in_specs=[on_chip] * 5,
        out_specs=(any_space,) * 5,
        scratch_shapes=[dma((5, 4))],
        compiler_params=pltpu.CompilerParams(vmem_limit_bytes=vmem_grant // 4),
    )(*(pltpu.with_memory_space_constraint(piece, pltpu.VMEM) for piece in fresh))
    return (new, copied, step, first_new, second_new)


def solution(mesh):
    line, plane, pair = (mesh.shape[name] for name in ("fs", "rep", "tp"))

    def chosen(*args):
        basis, first_moment = args[5], args[7]
        quarter_fits = first_moment.shape[0] % (plane * 128) == 0
        rows_fit = basis.shape[0] % (plane * 16) == 0 and basis.shape[0] % 64 == 0
        rank_fits = pair == 2 and first_moment.shape[1] % 128 == 0
        if line == 4 and plane == 4 and quarter_fits and rows_fit and rank_fits:
            return fast_body((line, plane), *args)
        return body(*args)

    return jax.shard_map(
        chosen,
        mesh=mesh,
        in_specs=(
            P(("fs", "rep"), "tp"),
            P(("fs", "rep"), "tp"),
            P("tp"),
            P(),
            P(("fs", "rep"), None),
            P("tp", None),
            P("tp", "fs"),
            P("fs", "tp"),
            P("fs", "tp"),
        ),
        out_specs=(P("tp", "fs"), P("tp", None), P("tp", "fs"), P("fs", "tp"), P("fs", "tp")),
        check_vma=False,
    )
```

time: 66.9 us -> 54.1 us (0.81)
  Pallas kernels: 66.1 us -> 53.3 us
    pallas_call x2, Pallas kernels: 66.1 us -> 53.3 us  [the longest x1 49.7 us: fast_body(): pl.pallas_call(functools.partial(exchange_kernel, sizes), out_shape=tuple...]
where the time goes in v1:
time: 54.1 us; the launch traced here: 54 us
  Pallas kernels  53.3 us (99%)
  between operations  0.64 us (1%)
    pallas_call x1, Pallas kernels, fast_body(): pl.pallas_call(functools.partial(exchange_kernel, sizes), out_shape=tuple...  49.7 us
    pallas_call x1, Pallas kernels, fast_body(): pl.pallas_call(store_kernel, out_shape=tuple((jax.ShapeDtypeStruct(shape,...  3.59 us

profile of v1, /device:TPU:0, one launch (start us, length us, event | category | flops | bytes accessed | tf_op | source)
XLA Modules:
  0.0 54.0 jit_solution(7732278440725041676)
XLA Ops:
  0.6 49.7 %shard_map.128 = (bf16[1024,2048]{1,0:T(8,128)(2,1)S(1)}, f32[1024,512]{1,0:T(8,128)S(1)}, f32[1024,512]{1,0:T(8,128)S(1)}, f32[512,128]{1,0:T(8,128)S(1)}, f32[512,128]{1,0:T(8,128)S(1)}) custom-call(f32[4]{0:T(128)} %lambda_ref.1, f32[1,256]{1,0:T(1,128)} %bitcast.1, bf16[768,1024]{1,0:T(8,128)(2,1)} %first_hbm.1, bf16[768,1024]{1,0:T(8,128)(2,1)} %second_hbm.1, ...), custom_call_target="tpu_custom_call" | custom-call | tf_op jit(solution)/shard_map/pallas_call | solution.py:597
  50.4 3.6 %shard_map.129 = (bf16[1024,2048]{1,0:T(8,128)(2,1)}, f32[1024,512]{1,0:T(8,128)}, f32[1024,512]{1,0:T(8,128)}, f32[512,128]{1,0:T(8,128)}, f32[512,128]{1,0:T(8,128)}) custom-call(bf16[1024,2048]{1,0:T(8,128)(2,1)S(1)} %get-tuple-element.15.refs_0_, f32[1024,512]{1,0:T(8,128)S(1)} %get-tuple-element.16.refs_1_, f32[1024,512]{1,0:T(8,128)S(1)} %get-tuple-element.17.refs_2_, ...), custom_call_target="tpu_custom_call" | custom-call | tf_op jit(solution)/shard_map/pallas_call | solution.py:661

commit v2 on v1

--- a/solution.py
+++ b/solution.py
@@ -15,6 +15,15 @@
 beta_second = 0.95
 quarter_chunks = 4
 extra_part = 8
+own, across = -1, -2
+plan = {
+    3: ((0, 1), (0, 2), (0, 3),),
+    7: ((own, 4), (own, 5), (1, 0), (1, 1),),
+    8: ((1, 2), (1, 3),),
+    11: ((across, 0), (2, 0), (2, 1), (2, 2), (2, 3), (0, 4), (0, 5),),
+    15: ((across, 1), (1, 4), (1, 5), (2, 4), (2, 5), (across, 2),),
+    16: ((0, 0),),
+}
 
 
 def head_output(first_piece, second_piece, lambdas, head_gain):
@@ -75,8 +84,8 @@
 
 def exchange_kernel(
     sizes,
-    lambda_ref,
-    gain_ref,
+    lambda_hbm,
+    gain_hbm,
     first_hbm,
     second_hbm,
     cot_hbm,
@@ -89,6 +98,8 @@
     step_ref,
     first_new_ref,
     second_new_ref,
+    lambda_ref,
+    gain_ref,
     first_v,
     second_v,
     cot_v,
@@ -111,6 +122,7 @@
     joined_v,
     load_sem,
     tile_sem,
+    ready_sem,
     wz_send,
     wf_send,
     wz_recv,
@@ -189,8 +201,12 @@
         pltpu.make_async_copy(moment1_hbm, moment1_v, load_sem.at[7]),
         pltpu.make_async_copy(moment2_hbm, moment2_v, load_sem.at[8]),
     ]
+    small_loads = [
+        pltpu.make_async_copy(lambda_hbm, lambda_ref, load_sem.at[9]),
+        pltpu.make_async_copy(gain_hbm, gain_ref, load_sem.at[10]),
+    ]
     weight_loads[0].start()
-    for load in basis_loads:
+    for load in small_loads + basis_loads:
         load.start()
     tile_loads = []
     for t in range(tiles):
@@ -207,17 +223,27 @@
     for load in moment_loads + weight_loads[2:]:
         load.start()
 
+    near_line = ((fs < line - 1, fs + 1), (fs > 0, fs - 1))
+    near_count = jnp.where((fs > 0) & (fs < line - 1), 2, 1)
+
+    def greet_line(semaphore):
+        for wanted, to in near_line:
+
+            @pl.when(wanted)
+            def _():
+                pl.semaphore_signal(
+                    semaphore, inc=1, device_id={"fs": to}, device_id_type=MESH
+                )
+
     barrier = pltpu.get_barrier_semaphore()
-    for step in range(1, line):
-        pl.semaphore_signal(
-            barrier, inc=1, device_id={"fs": lax.rem(fs + step, line)}, device_id_type=MESH
-        )
+    greet_line(barrier)
     for step in range(plane - 1):
         pl.semaphore_signal(
             barrier, inc=1, device_id={"rep": peers[step]}, device_id_type=MESH
         )
     pl.semaphore_signal(barrier, inc=1, device_id={"tp": other}, device_id_type=MESH)
-    pl.semaphore_wait(barrier, line + plane - 1)
+    pl.semaphore_wait(barrier, near_count + plane)
+    greet_line(ready_sem.at[0])
 
     sends = []
     guarded = []
@@ -299,12 +325,23 @@
         for side in range(2):
             relay_copy(t, side, far_side).wait_recv()
 
+    def weave(slot):
+        for step in plan.get(slot, ()):
+            if step[0] == own:
+                send_own(step[1])
+            elif step[0] == across:
+                relay(step[1])
+            else:
+                arrive(*step)
+
     weight_loads[0].wait()
     for c in quarters:
         narrow(c)
         send_own(c)
 
     for load in basis_loads:
+        load.wait()
+    for load in small_loads:
         load.wait()
     gain = gain_ref[...] * out_scale
     half_copies = []
@@ -342,9 +379,14 @@
         sends.append(copy)
         if t > 0:
             join_pair(t - 1)
+        if t == tiles - 2:
+            weave(0)
+    pl.semaphore_wait(ready_sem.at[0], near_count)
+    greet_line(ready_sem.at[1])
     cot_load.wait()
-    arrive(0, 0)
+    weave(16)
     join_pair(tiles - 1)
+    weave(1)
 
     order = (2, 1, 3, 0)
     plane_copies = {}
@@ -370,18 +412,20 @@
             copy.start()
             plane_copies[step, ahead] = copy
             sends.append(copy)
-
-    for c in quarters[1:]:
-        arrive(0, c)
+        if ahead == order[1]:
+            weave(2)
+
     weight_loads[1].wait()
     for c in extras:
         narrow(c)
+    weave(3)
     for load in moment_loads:
         load.wait()
     my_quarter = pl.ds(pl.multiple_of(rep * quarter, quarter), quarter)
     moment1 = moment1_v[my_quarter].T
     moment2 = moment2_v[my_quarter].T
 
+    pl.semaphore_wait(ready_sem.at[1], near_count)
     line_copies = []
     for ahead in order:
         total = mine_v[ahead, rep]
@@ -400,11 +444,7 @@
             copy.start()
             line_copies.append(copy)
             sends.append(copy)
-
-    for c in extras:
-        send_own(c)
-    for c in quarters[:2]:
-        arrive(1, c)
+        weave(4 + order.index(ahead))
 
     projected = total
     for copy, ahead in zip(line_copies, order):
@@ -457,25 +497,16 @@
         sends.append(copy)
         proj_copies.append(copy)
 
-    for c in quarters[2:]:
-        arrive(1, c)
+    weave(8)
     for at, source in enumerate(sources):
         spread_line(source, source, at).wait_recv()
         spread_plane(at, source)
-    relay(0)
-    for c in quarters:
-        arrive(2, c)
-    for c in extras:
-        arrive(0, c)
+        weave(9 + at)
     to_pair(3, fs)
+    weave(12)
     for at, source in enumerate(sources):
         to_pair(at, source)
-    relay(1)
-    for c in extras:
-        arrive(1, c)
-    for c in extras:
-        arrive(2, c)
-    relay(2)
+        weave(13 + at)
 
     for load in weight_loads[2:]:
         load.wait()
@@ -597,9 +628,11 @@
     fresh = pl.pallas_call(
         functools.partial(exchange_kernel, sizes),
         out_shape=tuple(pltpu.VMEM(shape, kind) for shape, kind in shapes),
-        in_specs=[pl.BlockSpec(memory_space=pltpu.SMEM), on_chip] + [any_space] * 7,
+        in_specs=[any_space] * 9,
         out_specs=(on_chip,) * 5,
         scratch_shapes=[
+            pltpu.SMEM(lambda_head.shape, f32),
+            pltpu.VMEM((1, head_gain.shape[0]), f32),
             pltpu.VMEM(first_mix.shape, bf16),
             pltpu.VMEM(second_mix.shape, bf16),
             pltpu.VMEM(out_cotangent.shape, bf16),
@@ -620,8 +653,9 @@
             pltpu.VMEM((plane, half, quarter), bf16),
             pltpu.VMEM((2, line, plane, half, quarter), bf16),
             pltpu.VMEM((rank, width), bf16),
-            dma((9,)),
+            dma((11,)),
             dma((tiles, 2)),
+            pltpu.SemaphoreType.REGULAR((2,)),
             dma((2, pieces)),
             dma((line - 1, pieces)),
             dma((line, pieces)),

time: 54.1 us -> 52.4 us (0.969)
  Pallas kernels: 53.3 us -> 51.6 us
    pallas_call x1, Pallas kernels: 49.7 us -> 48 us  [fast_body(): pl.pallas_call(functools.partial(exchange_kernel, sizes), out_shape=tuple...]
where the time goes in v2:
time: 52.4 us; the launch traced here: 52.2 us
  Pallas kernels  51.6 us (98%)
  between operations  0.64 us (1%)
    pallas_call x1, Pallas kernels, fast_body(): pl.pallas_call(functools.partial(exchange_kernel, sizes), out_shape=tuple...  48 us
    pallas_call x1, Pallas kernels, fast_body(): pl.pallas_call(store_kernel, out_shape=tuple((jax.ShapeDtypeStruct(shape,...  3.59 us

profile of v2, /device:TPU:0, one launch (start us, length us, event | category | flops | bytes accessed | tf_op | source)
XLA Modules:
  0.0 52.2 jit_solution(4846652460001957571)
XLA Ops:
  0.6 48.0 %shard_map.128 = (bf16[1024,2048]{1,0:T(8,128)(2,1)S(1)}, f32[1024,512]{1,0:T(8,128)S(1)}, f32[1024,512]{1,0:T(8,128)S(1)}, f32[512,128]{1,0:T(8,128)S(1)}, f32[512,128]{1,0:T(8,128)S(1)}) custom-call(f32[4]{0:T(128)} %lambda_hbm.1, f32[1,256]{1,0:T(1,128)} %bitcast.1, bf16[768,1024]{1,0:T(8,128)(2,1)} %first_hbm.1, bf16[768,1024]{1,0:T(8,128)(2,1)} %second_hbm.1, ...), custom_call_target="tpu_custom_call" | custom-call | tf_op jit(solution)/shard_map/pallas_call | solution.py:628
  48.6 3.6 %shard_map.129 = (bf16[1024,2048]{1,0:T(8,128)(2,1)}, f32[1024,512]{1,0:T(8,128)}, f32[1024,512]{1,0:T(8,128)}, f32[512,128]{1,0:T(8,128)}, f32[512,128]{1,0:T(8,128)}) custom-call(bf16[1024,2048]{1,0:T(8,128)(2,1)S(1)} %get-tuple-element.15.refs_0_, f32[1024,512]{1,0:T(8,128)S(1)} %get-tuple-element.16.refs_1_, f32[1024,512]{1,0:T(8,128)S(1)} %get-tuple-element.17.refs_2_, ...), custom_call_target="tpu_custom_call" | custom-call | tf_op jit(solution)/shard_map/pallas_call | solution.py:695

commit v3 on v2

--- a/solution.py
+++ b/solution.py
@@ -14,15 +14,28 @@
 beta_first = 0.9
 beta_second = 0.95
 quarter_chunks = 4
-extra_part = 8
-own, across = -1, -2
+extra_part = 10
+own, across, turned, kept = -1, -2, -3, -4
 plan = {
-    3: ((0, 1), (0, 2), (0, 3),),
-    7: ((own, 4), (own, 5), (1, 0), (1, 1),),
-    8: ((1, 2), (1, 3),),
-    11: ((across, 0), (2, 0), (2, 1), (2, 2), (2, 3), (0, 4), (0, 5),),
-    15: ((across, 1), (1, 4), (1, 5), (2, 4), (2, 5), (across, 2),),
-    16: ((0, 0),),
+    16: ((own, 5),),
+    17: ((own, 4), (0, 0),),
+    4: ((0, 2),),
+    6: ((0, 3),),
+    7: ((0, 1), (1, 2),),
+    8: ((kept,), (turned, 3), (1, 3), (0, 4),),
+    11: (
+        (1, 0),
+        (2, 2),
+        (turned, 1),
+        (2, 3),
+        (turned, 2),
+        (1, 4),
+        (turned, 0),
+        (across, 1),
+        (0, 5),
+    ),
+    12: ((1, 1), (2, 0), (across, 0), (1, 5), (2, 4), (2, 1), (across, 2),),
+    15: ((2, 5),),
 }
 
 
@@ -113,8 +126,10 @@
     half_recv_v,
     turned_v,
     mine_v,
-    plane_send_v,
-    plane_recv_v,
+    across_send_v,
+    across_recv_v,
+    joint_send_v,
+    joint_recv_v,
     line_send_v,
     line_recv_v,
     projected_v,
@@ -132,8 +147,10 @@
     wr_recv,
     half_send,
     half_recv,
-    plane_send,
-    plane_recv,
+    across_send,
+    across_recv,
+    joint_send,
+    joint_recv,
     line_send,
     line_recv,
     proj_send,
@@ -142,6 +159,8 @@
     dz_recv,
     dp_send,
     dp_recv,
+    dr_send,
+    dr_recv,
     dt_send,
     dt_recv,
 ):
@@ -313,7 +332,9 @@
 
     def relay(t):
         for side in range(2):
-            from_side(t, (extra + side * rest) // chunk, side)
+            start = extra + side * rest
+            for c in range(start // chunk, -(-(start + rest) // chunk)):
+                from_side(t, c, side)
             copy = relay_copy(t, side, sides[side])
             copy.start()
             sends.append(copy)
@@ -331,6 +352,10 @@
                 send_own(step[1])
             elif step[0] == across:
                 relay(step[1])
+            elif step[0] == turned:
+                relay_direction(step[1])
+            elif step[0] == kept:
+                spread_projected()
             else:
                 arrive(*step)
 
@@ -383,13 +408,20 @@
             weave(0)
     pl.semaphore_wait(ready_sem.at[0], near_count)
     greet_line(ready_sem.at[1])
+    weight_loads[1].wait()
+    for c in extras:
+        narrow(c)
     cot_load.wait()
     weave(16)
     join_pair(tiles - 1)
     weave(1)
 
     order = (2, 1, 3, 0)
-    plane_copies = {}
+    middle = half // 2
+    halves = (pl.ds(0, middle), pl.ds(middle, middle))
+    bits = (lax.rem(rep, 2), lax.div(rep, 2))
+    across_copies = {}
+    joint_copies = {}
     for ahead in order:
         at = lax.rem(fs + ahead, line)
         product = jnp.dot(
@@ -400,24 +432,23 @@
         for part in range(plane):
             piece = product[:, part * quarter : (part + 1) * quarter]
             mine_v[ahead, part] = piece
-            plane_send_v[ahead, part] = piece.astype(jnp.bfloat16)
-        for step in range(plane - 1):
+            piece = piece.astype(jnp.bfloat16)
+            across_send_v[0, ahead, part % 2, part // 2] = piece[:middle]
+            across_send_v[1, ahead, part // 2, part % 2] = piece[middle:]
+        for side in range(2):
             copy = remote(
-                plane_send_v.at[ahead, peers[step]],
-                plane_recv_v.at[step, ahead],
-                plane_send.at[step, ahead],
-                plane_recv.at[step, ahead],
-                {"rep": peers[step]},
+                across_send_v.at[side, ahead, 1 - bits[side]],
+                across_recv_v.at[side, ahead],
+                across_send.at[side, ahead],
+                across_recv.at[side, ahead],
+                {"rep": sides[side]},
             )
             copy.start()
-            plane_copies[step, ahead] = copy
+            across_copies[side, ahead] = copy
             sends.append(copy)
         if ahead == order[1]:
             weave(2)
 
-    weight_loads[1].wait()
-    for c in extras:
-        narrow(c)
     weave(3)
     for load in moment_loads:
         load.wait()
@@ -425,13 +456,38 @@
     moment1 = moment1_v[my_quarter].T
     moment2 = moment2_v[my_quarter].T
 
+    for ahead in order:
+        for side in range(2):
+            across_copies[side, ahead].wait_recv()
+            turn = 1 - side
+            joint = (
+                mine_v[ahead, sides[turn], halves[side]]
+                + across_recv_v[side, ahead, 1 - bits[turn]].astype(jnp.float32)
+            )
+            joint_send_v[side, ahead] = joint.astype(jnp.bfloat16)
+            copy = remote(
+                joint_send_v.at[side, ahead],
+                joint_recv_v.at[side, ahead],
+                joint_send.at[side, ahead],
+                joint_recv.at[side, ahead],
+                {"rep": sides[turn]},
+            )
+            copy.start()
+            joint_copies[side, ahead] = copy
+            sends.append(copy)
+        weave(17 + order.index(ahead))
     pl.semaphore_wait(ready_sem.at[1], near_count)
     line_copies = []
     for ahead in order:
-        total = mine_v[ahead, rep]
-        for step in range(plane - 1):
-            plane_copies[step, ahead].wait_recv()
-            total = total + plane_recv_v[step, ahead].astype(jnp.float32)
+        totals = []
+        for side in range(2):
+            joint_copies[side, ahead].wait_recv()
+            totals.append(
+                mine_v[ahead, rep, halves[side]]
+                + across_recv_v[side, ahead, bits[1 - side]].astype(jnp.float32)
+                + joint_recv_v[side, ahead].astype(jnp.float32)
+            )
+        total = jnp.concatenate(totals, axis=0)
         if ahead:
             line_send_v[ahead] = total.astype(jnp.bfloat16)
             copy = remote(
@@ -460,23 +516,34 @@
         here = direction_v.at[tp, source, rep]
         return remote(here, here, dz_send.at[at], dz_recv.at[source], {"fs": to})
 
-    plane_directions = {}
-
     def spread_plane(at, source):
-        for step in range(plane - 1):
+        for side in range(2):
             here = direction_v.at[tp, source, rep]
             copy = remote(
-                here, here, dp_send.at[at, step], dp_recv.at[at, step], {"rep": peers[step]}
+                here, here, dp_send.at[at, side], dp_recv.at[at, side], {"rep": sides[side]}
             )
             copy.start()
             sends.append(copy)
 
+    def spread_relay_copy(at, side, owner):
+        here = direction_v.at[tp, (sources + (fs,))[at], owner, halves[side]]
+        return remote(
+            here, here, dr_send.at[at, side], dr_recv.at[at, side], {"rep": sides[1 - side]}
+        )
+
+    def relay_direction(at):
+        for side in range(2):
+            here = direction_v.at[tp, (sources + (fs,))[at], sides[side]]
+            remote(
+                here, here, dp_send.at[at, side], dp_recv.at[at, side], {"rep": sides[side]}
+            ).wait_recv()
+            copy = spread_relay_copy(at, side, sides[side])
+            copy.start()
+            sends.append(copy)
+
     def to_pair(at, source):
-        for step in range(plane - 1):
-            here = direction_v.at[tp, source, peers[step]]
-            remote(
-                here, here, dp_send.at[at, step], dp_recv.at[at, step], {"rep": peers[step]}
-            ).wait_recv()
+        for side in range(2):
+            spread_relay_copy(at, side, far_side).wait_recv()
         here = direction_v.at[tp, source]
         copy = remote(here, here, dt_send.at[at], dt_recv.at[at], {"tp": other})
         copy.start()
@@ -488,14 +555,16 @@
         sends.append(copy)
     spread_plane(3, fs)
     proj_copies = []
-    for step in range(plane - 1):
-        here = projected_v.at[rep]
-        copy = remote(
-            here, here, proj_send.at[step], proj_recv.at[step], {"rep": peers[step]}
-        )
-        copy.start()
-        sends.append(copy)
-        proj_copies.append(copy)
+
+    def spread_projected():
+        for step in range(plane - 1):
+            here = projected_v.at[rep]
+            copy = remote(
+                here, here, proj_send.at[step], proj_recv.at[step], {"rep": peers[step]}
+            )
+            copy.start()
+            sends.append(copy)
+            proj_copies.append(copy)
 
     weave(8)
     for at, source in enumerate(sources):
@@ -508,8 +577,6 @@
         to_pair(at, source)
         weave(13 + at)
 
-    for load in weight_loads[2:]:
-        load.wait()
     for at, source in enumerate(sources + (fs,)):
         here = direction_v.at[other, source]
         remote(here, here, dt_send.at[at], dt_recv.at[at], {"tp": other}).wait_recv()
@@ -525,6 +592,7 @@
     total = jnp.sum(jnp.sum(energy, axis=0, keepdims=True), axis=1, keepdims=True)
     spread = jnp.sqrt(total / (width * 2 * half))
     scale = -1.0 / (spread + 1e-06)
+    weave(21)
 
     block = values // 4
 
@@ -541,6 +609,8 @@
     def columns_of(at):
         return pl.ds(pl.multiple_of(at * shard, shard), shard)
 
+    for load in weight_loads[2:]:
+        load.wait()
     for b in range(4):
         rows = pl.ds(b * block, block)
         step = step_block(fs, rows)
@@ -557,6 +627,7 @@
         second_new_ref[rows, :] = (
             beta_second * moment2_v[rows, :] + (1.0 - beta_second) * piece * piece
         )
+    weave(22)
     for t, source in enumerate(sources):
         finish(t)
         for b in range(4):
@@ -564,6 +635,7 @@
             copy_ref[rows, columns_of(source)] = (
                 gathered_v[source, rows].astype(jnp.float32) + step_block(source, rows)
             ).astype(jnp.bfloat16)
+        weave(23 + t)
     for copy in sends:
         copy.wait_send()
     for wanted, copy in guarded:
@@ -646,8 +718,10 @@
             pltpu.VMEM((tiles, tile, half), f32),
             pltpu.VMEM((half, tokens), bf16),
             pltpu.VMEM((line, plane, half, quarter), f32),
-            pltpu.VMEM((line, plane, half, quarter), bf16),
-            pltpu.VMEM((plane - 1, line, half, quarter), bf16),
+            pltpu.VMEM((2, line, 2, 2, half // 2, quarter), bf16),
+            pltpu.VMEM((2, line, 2, half // 2, quarter), bf16),
+            pltpu.VMEM((2, line, half // 2, quarter), bf16),
+            pltpu.VMEM((2, line, half // 2, quarter), bf16),
             pltpu.VMEM((line, half, quarter), bf16),
             pltpu.VMEM((line, half, quarter), bf16),
             pltpu.VMEM((plane, half, quarter), bf16),
@@ -665,16 +739,20 @@
             dma((line - 1, 2)),
             dma((tiles,)),
             dma((tiles,)),
-            dma((plane - 1, line)),
-            dma((plane - 1, line)),
+            dma((2, line)),
+            dma((2, line)),
+            dma((2, line)),
+            dma((2, line)),
             dma((line,)),
             dma((line,)),
             dma((plane - 1,)),
             dma((plane - 1,)),
             dma((line - 1,)),
             dma((line,)),
-            dma((line, plane - 1)),
-            dma((line, plane - 1)),
+            dma((line, 2)),
+            dma((line, 2)),
+            dma((line, 2)),
+            dma((line, 2)),
             dma((line,)),
             dma((line,)),
         ],

time: 52.4 us -> 49.8 us (0.950)
  Pallas kernels: 51.6 us -> 49 us
    pallas_call x1, Pallas kernels: 48 us -> 45.4 us  [fast_body(): pl.pallas_call(functools.partial(exchange_kernel, sizes), out_shape=tuple...]
where the time goes in v3:
time: 49.8 us; the launch traced here: 49.7 us
  Pallas kernels  49 us (98%)
  between operations  0.64 us (1%)
    pallas_call x1, Pallas kernels, fast_body(): pl.pallas_call(functools.partial(exchange_kernel, sizes), out_shape=tuple...  45.4 us
    pallas_call x1, Pallas kernels, fast_body(): pl.pallas_call(store_kernel, out_shape=tuple((jax.ShapeDtypeStruct(shape,...  3.59 us

profile of v3, /device:TPU:0, one launch (start us, length us, event | category | flops | bytes accessed | tf_op | source)
XLA Modules:
  0.0 49.7 jit_solution(16447421563839138537)
XLA Ops:
  0.6 45.4 %shard_map.128 = (bf16[1024,2048]{1,0:T(8,128)(2,1)S(1)}, f32[1024,512]{1,0:T(8,128)S(1)}, f32[1024,512]{1,0:T(8,128)S(1)}, f32[512,128]{1,0:T(8,128)S(1)}, f32[512,128]{1,0:T(8,128)S(1)}) custom-call(f32[4]{0:T(128)} %lambda_hbm.1, f32[1,256]{1,0:T(1,128)} %bitcast.1, bf16[768,1024]{1,0:T(8,128)(2,1)} %first_hbm.1, bf16[768,1024]{1,0:T(8,128)(2,1)} %second_hbm.1, ...), custom_call_target="tpu_custom_call" | custom-call | tf_op jit(solution)/shard_map/pallas_call | solution.py:700
  46.1 3.6 %shard_map.129 = (bf16[1024,2048]{1,0:T(8,128)(2,1)}, f32[1024,512]{1,0:T(8,128)}, f32[1024,512]{1,0:T(8,128)}, f32[512,128]{1,0:T(8,128)}, f32[512,128]{1,0:T(8,128)}) custom-call(bf16[1024,2048]{1,0:T(8,128)(2,1)S(1)} %get-tuple-element.15.refs_0_, f32[1024,512]{1,0:T(8,128)S(1)} %get-tuple-element.16.refs_1_, f32[1024,512]{1,0:T(8,128)S(1)} %get-tuple-element.17.refs_2_, ...), custom_call_target="tpu_custom_call" | custom-call | tf_op jit(solution)/shard_map/pallas_call | solution.py:773

commit v4 on v3

--- a/solution.py
+++ b/solution.py
@@ -24,13 +24,13 @@
     7: ((0, 1), (1, 2),),
     8: ((kept,), (turned, 3), (1, 3), (0, 4),),
     11: (
+        (1, 4),
         (1, 0),
         (2, 2),
         (turned, 1),
         (2, 3),
+        (turned, 0),
         (turned, 2),
-        (1, 4),
-        (turned, 0),
         (across, 1),
         (0, 5),
     ),
@@ -237,10 +237,6 @@
         for piece in pieces:
             piece.start()
         tile_loads.append(pieces)
-    cot_load.start()
-    weight_loads[1].start()
-    for load in moment_loads + weight_loads[2:]:
-        load.start()
 
     near_line = ((fs < line - 1, fs + 1), (fs > 0, fs - 1))
     near_count = jnp.where((fs > 0) & (fs < line - 1), 2, 1)
@@ -360,6 +356,10 @@
                 arrive(*step)
 
     weight_loads[0].wait()
+    cot_load.start()
+    weight_loads[1].start()
+    for load in moment_loads + weight_loads[2:]:
+        load.start()
     for c in quarters:
         narrow(c)
         send_own(c)
@@ -775,7 +775,7 @@
         out_shape=tuple(jax.ShapeDtypeStruct(shape, kind) for shape, kind in shapes),
         in_specs=[on_chip] * 5,
         out_specs=(any_space,) * 5,
-        scratch_shapes=[dma((5, 4))],
+        scratch_shapes=[dma((5, 1))],
         compiler_params=pltpu.CompilerParams(vmem_limit_bytes=vmem_grant // 4),
     )(*(pltpu.with_memory_space_constraint(piece, pltpu.VMEM) for piece in fresh))
     return (new, copied, step, first_new, second_new)

time: 49.8 us -> 48.2 us (0.968)
  Pallas kernels: 49 us -> 47.4 us
    pallas_call x1, Pallas kernels: 45.4 us -> 43.9 us  [fast_body(): pl.pallas_call(functools.partial(exchange_kernel, sizes), out_shape=tuple...]
where the time goes in v4:
time: 48.2 us; the launch traced here: 48 us
  Pallas kernels  47.4 us (98%)
  between operations  0.64 us (1%)
    pallas_call x1, Pallas kernels, fast_body(): pl.pallas_call(functools.partial(exchange_kernel, sizes), out_shape=tuple...  43.9 us
    pallas_call x1, Pallas kernels, fast_body(): pl.pallas_call(store_kernel, out_shape=tuple((jax.ShapeDtypeStruct(shape,...  3.47 us

profile of v4, /device:TPU:0, one launch (start us, length us, event | category | flops | bytes accessed | tf_op | source)
XLA Modules:
  0.0 48.0 jit_solution(2843876154817669084)
XLA Ops:
  0.6 43.9 %shard_map.128 = (bf16[1024,2048]{1,0:T(8,128)(2,1)S(1)}, f32[1024,512]{1,0:T(8,128)S(1)}, f32[1024,512]{1,0:T(8,128)S(1)}, f32[512,128]{1,0:T(8,128)S(1)}, f32[512,128]{1,0:T(8,128)S(1)}) custom-call(f32[4]{0:T(128)} %lambda_hbm.1, f32[1,256]{1,0:T(1,128)} %bitcast.1, bf16[768,1024]{1,0:T(8,128)(2,1)} %first_hbm.1, bf16[768,1024]{1,0:T(8,128)(2,1)} %second_hbm.1, ...), custom_call_target="tpu_custom_call" | custom-call | tf_op jit(solution)/shard_map/pallas_call | solution.py:700
  44.6 3.5 %shard_map.129 = (bf16[1024,2048]{1,0:T(8,128)(2,1)}, f32[1024,512]{1,0:T(8,128)}, f32[1024,512]{1,0:T(8,128)}, f32[512,128]{1,0:T(8,128)}, f32[512,128]{1,0:T(8,128)}) custom-call(bf16[1024,2048]{1,0:T(8,128)(2,1)S(1)} %get-tuple-element.15.refs_0_, f32[1024,512]{1,0:T(8,128)S(1)} %get-tuple-element.16.refs_1_, f32[1024,512]{1,0:T(8,128)S(1)} %get-tuple-element.17.refs_2_, ...), custom_call_target="tpu_custom_call" | custom-call | tf_op jit(solution)/shard_map/pallas_call | solution.py:773

commit v5 on v4

--- a/solution.py
+++ b/solution.py
@@ -15,25 +15,16 @@
 beta_second = 0.95
 quarter_chunks = 4
 extra_part = 10
-own, across, turned, kept = -1, -2, -3, -4
+own, across, turned = -1, -2, -3
 plan = {
     16: ((own, 5),),
     17: ((own, 4), (0, 0),),
     4: ((0, 2),),
     6: ((0, 3),),
     7: ((0, 1), (1, 2),),
-    8: ((kept,), (turned, 3), (1, 3), (0, 4),),
-    11: (
-        (1, 4),
-        (1, 0),
-        (2, 2),
-        (turned, 1),
-        (2, 3),
-        (turned, 0),
-        (turned, 2),
-        (across, 1),
-        (0, 5),
-    ),
+    8: ((0, 4), (1, 0), (1, 3),),
+    10: ((turned, 3),),
+    11: ((1, 4), (2, 2), (turned, 1), (2, 3), (turned, 0), (turned, 2), (across, 1), (0, 5),),
     12: ((1, 1), (2, 0), (across, 0), (1, 5), (2, 4), (2, 1), (across, 2),),
     15: ((2, 5),),
 }
@@ -153,8 +144,6 @@
     joint_recv,
     line_send,
     line_recv,
-    proj_send,
-    proj_recv,
     dz_send,
     dz_recv,
     dp_send,
@@ -350,8 +339,6 @@
                 relay(step[1])
             elif step[0] == turned:
                 relay_direction(step[1])
-            elif step[0] == kept:
-                spread_projected()
             else:
                 arrive(*step)
 
@@ -506,19 +493,29 @@
     for copy, ahead in zip(line_copies, order):
         copy.wait_recv()
         projected = projected + line_recv_v[ahead].astype(jnp.float32)
-    first_new = beta_first * moment1 + (1.0 - beta_first) * projected
-    second_new = beta_second * moment2 + (1.0 - beta_second) * projected * projected
-    direction = first_new / (jnp.sqrt(second_new) + 1e-08)
-    direction_v[tp, fs, rep] = direction.astype(jnp.bfloat16)
     projected_v[rep] = projected.astype(jnp.bfloat16)
+
+    def settle(part, moment1, moment2):
+        wide = projected_v[part].astype(jnp.float32)
+        first_new = beta_first * moment1 + (1.0 - beta_first) * wide
+        second_new = beta_second * moment2 + (1.0 - beta_second) * wide * wide
+        direction = first_new / (jnp.sqrt(second_new) + 1e-08)
+        direction_v[tp, fs, part] = direction.astype(jnp.bfloat16)
+
+    settle(rep, moment1, moment2)
 
     def spread_line(source, to, at):
         here = direction_v.at[tp, source, rep]
         return remote(here, here, dz_send.at[at], dz_recv.at[source], {"fs": to})
 
-    def spread_plane(at, source):
+    def piece_of(at, *where):
+        if at == line - 1:
+            return projected_v.at[where]
+        return direction_v.at[(tp, sources[at]) + where]
+
+    def spread_plane(at):
         for side in range(2):
-            here = direction_v.at[tp, source, rep]
+            here = piece_of(at, rep)
             copy = remote(
                 here, here, dp_send.at[at, side], dp_recv.at[at, side], {"rep": sides[side]}
             )
@@ -526,14 +523,14 @@
             sends.append(copy)
 
     def spread_relay_copy(at, side, owner):
-        here = direction_v.at[tp, (sources + (fs,))[at], owner, halves[side]]
+        here = piece_of(at, owner, halves[side])
         return remote(
             here, here, dr_send.at[at, side], dr_recv.at[at, side], {"rep": sides[1 - side]}
         )
 
     def relay_direction(at):
         for side in range(2):
-            here = direction_v.at[tp, (sources + (fs,))[at], sides[side]]
+            here = piece_of(at, sides[side])
             remote(
                 here, here, dp_send.at[at, side], dp_recv.at[at, side], {"rep": sides[side]}
             ).wait_recv()
@@ -544,6 +541,10 @@
     def to_pair(at, source):
         for side in range(2):
             spread_relay_copy(at, side, far_side).wait_recv()
+        if at == line - 1:
+            for part in peers[:-1]:
+                rows = pl.ds(pl.multiple_of(part * quarter, quarter), quarter)
+                settle(part, moment1_v[rows].T, moment2_v[rows].T)
         here = direction_v.at[tp, source]
         copy = remote(here, here, dt_send.at[at], dt_recv.at[at], {"tp": other})
         copy.start()
@@ -553,23 +554,11 @@
         copy = spread_line(fs, to, at)
         copy.start()
         sends.append(copy)
-    spread_plane(3, fs)
-    proj_copies = []
-
-    def spread_projected():
-        for step in range(plane - 1):
-            here = projected_v.at[rep]
-            copy = remote(
-                here, here, proj_send.at[step], proj_recv.at[step], {"rep": peers[step]}
-            )
-            copy.start()
-            sends.append(copy)
-            proj_copies.append(copy)
-
+    spread_plane(3)
     weave(8)
     for at, source in enumerate(sources):
         spread_line(source, source, at).wait_recv()
-        spread_plane(at, source)
+        spread_plane(at)
         weave(9 + at)
     to_pair(3, fs)
     weave(12)
@@ -618,8 +607,6 @@
         step_ref[rows, :] = step
         new_ref[rows, :] = fresh
         copy_ref[rows, columns_of(fs)] = fresh.astype(jnp.bfloat16)
-    for copy in proj_copies:
-        copy.wait_recv()
     for part in range(plane):
         rows = pl.ds(part * quarter, quarter)
         piece = projected_v[part].astype(jnp.float32).T
@@ -745,8 +732,6 @@
             dma((2, line)),
             dma((line,)),
             dma((line,)),
-            dma((plane - 1,)),
-            dma((plane - 1,)),
             dma((line - 1,)),
             dma((line,)),
             dma((line, 2)),

time: 48.2 us -> 47.5 us (0.985)
  Pallas kernels: 47.4 us -> 46.7 us
    pallas_call x1, Pallas kernels: 43.9 us -> 43.2 us  [fast_body(): pl.pallas_call(functools.partial(exchange_kernel, sizes), out_shape=tuple...]
where the time goes in v5:
time: 47.5 us; the launch traced here: 47.3 us
  Pallas kernels  46.7 us (98%)
  between operations  0.64 us (1%)
    pallas_call x1, Pallas kernels, fast_body(): pl.pallas_call(functools.partial(exchange_kernel, sizes), out_shape=tuple...  43.2 us
    pallas_call x1, Pallas kernels, fast_body(): pl.pallas_call(store_kernel, out_shape=tuple((jax.ShapeDtypeStruct(shape,...  3.47 us

profile of v5, /device:TPU:0, one launch (start us, length us, event | category | flops | bytes accessed | tf_op | source)
XLA Modules:
  0.0 47.3 jit_solution(12977382664343266018)
XLA Ops:
  0.6 43.2 %shard_map.128 = (bf16[1024,2048]{1,0:T(8,128)(2,1)S(1)}, f32[1024,512]{1,0:T(8,128)S(1)}, f32[1024,512]{1,0:T(8,128)S(1)}, f32[512,128]{1,0:T(8,128)S(1)}, f32[512,128]{1,0:T(8,128)S(1)}) custom-call(f32[4]{0:T(128)} %lambda_hbm.1, f32[1,256]{1,0:T(1,128)} %bitcast.1, bf16[768,1024]{1,0:T(8,128)(2,1)} %first_hbm.1, bf16[768,1024]{1,0:T(8,128)(2,1)} %second_hbm.1, ...), custom_call_target="tpu_custom_call" | custom-call | tf_op jit(solution)/shard_map/pallas_call | solution.py:687
  43.9 3.5 %shard_map.129 = (bf16[1024,2048]{1,0:T(8,128)(2,1)}, f32[1024,512]{1,0:T(8,128)}, f32[1024,512]{1,0:T(8,128)}, f32[512,128]{1,0:T(8,128)}, f32[512,128]{1,0:T(8,128)}) custom-call(bf16[1024,2048]{1,0:T(8,128)(2,1)S(1)} %get-tuple-element.15.refs_0_, f32[1024,512]{1,0:T(8,128)S(1)} %get-tuple-element.16.refs_1_, f32[1024,512]{1,0:T(8,128)S(1)} %get-tuple-element.17.refs_2_, ...), custom_call_target="tpu_custom_call" | custom-call | tf_op jit(solution)/shard_map/pallas_call | solution.py:758
